TPU v7x, 32 devices: a whole 2x2x4 slice. The times are simulated.
32 devices in a mesh: sp: 8 (over z, x), tp: 4 (over y, core).
Axes of the slice: x: 2, y: 2, z: 4, core: 2. Of those that a mesh axis runs over, the one named last changes fastest.
Arguments:
- resid: bfloat16 [4096, 2048], P(('sp', 'tp')), may hold values from -6 to 6
- pool_in: bfloat16 [4096, 1024], P('sp', 'tp'), may hold values from -8 to 8
- doc_ids: int32 [4096], P('sp'), may hold values from 0 to 3, never falling along the last dimension, each value on 1 to 1536 neighbouring positions
- w_group: bfloat16 [8, 128, 128], replicated, may hold values from -0.5 to 0.5
- pool_scale: bfloat16 [1024], replicated, may hold values from 0.099609375 to 1.8984375
- w_branch: bfloat16 [1024, 2048], P('tp'), may hold values from -0.1875 to 0.1875
- norm_gain: bfloat16 [2048], replicated, may hold values from 0.099609375 to 1.8984375
- route_ids: int32 [4096, 4], P(('sp', 'tp')), may hold values from 0 to 31, all different within a row; in each aligned block of 128 rows (0 to 127, 128 to 255, ...) at most 32 rows name the same one
- route_wts: float32 [4096, 4], P(('sp', 'tp')), may hold values from 0.2 to 1
- w_exp_gate: bfloat16 [32, 2048, 512], P(('sp', 'tp')), may hold values from -0.125 to 0.125
- w_exp_up: bfloat16 [32, 2048, 512], P(('sp', 'tp')), may hold values from -0.125 to 0.125
- w_exp_down: bfloat16 [32, 512, 2048], P(('sp', 'tp')), may hold values from -0.25 to 0.25
- w_sh_gate: bfloat16 [2048, 512], replicated, may hold values from -0.125 to 0.125
- w_sh_up: bfloat16 [2048, 512], replicated, may hold values from -0.125 to 0.125
- w_sh_down: bfloat16 [512, 2048], replicated, may hold values from -0.25 to 0.25
- final_gain: bfloat16 [2048], replicated, may hold values from 0.099609375 to 1.8984375
Outputs:
- final: bfloat16 [4096, 2048], P(('sp', 'tp'))
Inputs may be any that keep to these rules, and one draw needn't show every extreme that they name: `doc_ids`: never falls along the positions. `route_ids`: each row names 4 different experts; among the rows of one device (aligned blocks of 128 rows) no expert is named by more than 32 rows, a bound that some block reaches.
All inputs are finite; a program needn't handle non-finite values.
Results may differ from a plain program's by a relative error of at most 0.0062.
Values may be sent and summed in bfloat16 or wider, within the bound.
A program may use at most 128 MiB of HBM per device.

v0:
```python
import functools

import jax
import jax.numpy as jnp
from jax import lax
from jax.experimental import pallas as pl
from jax.experimental.pallas import tpu as pltpu
from jax.sharding import PartitionSpec as P

pool_windows = (2, 4, 8, 16, 16, 32, 64, 128)
alpha_mix = 8.0**0.25
norm_eps = 1e-05
halo = max(pool_windows)
MESH = pl.DeviceIdType.MESH
wb_chunks = 4


def layer_norm(values, gain):
    center = values - jnp.mean(values, axis=-1, keepdims=True)
    spread = jnp.mean(center * center, axis=-1, keepdims=True)
    return center * lax.rsqrt(spread + norm_eps) * gain.astype(jnp.float32)


def dot(a, b):
    return jnp.dot(a, b, preferred_element_type=jnp.float32)


def silu_mul(gate, up):
    return (gate / (1.0 + jnp.exp(-gate)) * up).astype(jnp.bfloat16)


def pool_kernel(
    n_sp, n_tp,
    pool_ref, docc_ref, docr_ref, wg_ref, scale_ref, wb_ref, resid_ref, gain_ref, meta_ref,
    out_ref, metas_ref,
    ext, stats, mixed, token_rows, wb_all,
    stat_send, stat_recv, halo_send, halo_recv, mix_send, mix_recv,
    wb_send, wb_recv, fw_send, wb_local,
):
    s, p = lax.axis_index("sp"), lax.axis_index("tp")
    toks, width = pool_ref.shape
    group_width = wg_ref.shape[1]
    rows = resid_ref.shape[0]
    depth = wb_ref.shape[0]
    piece = depth // wb_chunks
    partner = p + 1 - 2 * lax.rem(p, 2)

    barrier = pltpu.get_barrier_semaphore()
    for k in range(1, n_sp):
        pl.semaphore_signal(barrier, inc=1, device_id=(lax.rem(s + k, n_sp), p), device_id_type=MESH)
    for k in range(1, n_tp):
        pl.semaphore_signal(barrier, inc=1, device_id=(s, lax.rem(p + k, n_tp)), device_id_type=MESH)
    pl.semaphore_wait(barrier, n_sp + n_tp - 2)

    def wb_copy(c, src, slot, target, send, recv):
        window = pl.ds(c * piece, piece)
        return pltpu.make_async_remote_copy(
            src_ref=src.at[window], dst_ref=wb_all.at[slot, window],
            send_sem=send, recv_sem=recv, device_id=(s, target), device_id_type=MESH,
        )

    own_wb = pltpu.make_async_copy(wb_ref, wb_all.at[p], wb_local)
    own_wb.start()

    values = pool_ref[...]
    docc, docr = docc_ref[...], docr_ref[...]
    last = jnp.max(docr, axis=1, keepdims=True)
    first = jnp.min(docr, axis=1, keepdims=True).astype(jnp.float32)
    tail = (docr == last).astype(jnp.float32)
    tail_count = jnp.sum(tail, axis=1, keepdims=True)
    sums = dot(jnp.broadcast_to(tail, (8, toks)).astype(jnp.bfloat16), values)
    lane = lax.broadcasted_iota(jnp.int32, (8, 128), 1)
    stats[s, :, 0:width] = sums
    stats[s, :, width + 128 :] = meta_ref[...]
    stats[s, :, width : width + 128] = jnp.where(lane == 0, last.astype(jnp.float32), tail_count)

    halo_copy = pltpu.make_async_remote_copy(
        src_ref=pool_ref.at[pl.ds(toks - halo, halo)], dst_ref=ext.at[pl.ds(0, halo)],
        send_sem=halo_send, recv_sem=halo_recv,
        device_id=(lax.rem(s + 1, n_sp), p), device_id_type=MESH,
    )
    halo_copy.start()
    ext[halo:, :] = values

    tpos = lax.broadcasted_iota(jnp.int32, (toks, toks), 0)
    spos = lax.broadcasted_iota(jnp.int32, (toks, toks), 1)
    same = ((docc == docr) & (spos <= tpos)).astype(jnp.float32)
    here = jnp.sum(same, axis=1, keepdims=True)
    running = dot(same.astype(jnp.bfloat16), values)

    stat_copies = []
    for k in range(1, n_sp):
        stat_copies.append(
            pltpu.make_async_remote_copy(
                src_ref=stats.at[s], dst_ref=stats.at[s],
                send_sem=stat_send.at[k], recv_sem=stat_recv.at[k],
                device_id=(lax.rem(s + k, n_sp), p), device_id_type=MESH,
            )
        )
        stat_copies[-1].start()

    cross = []
    for c in range(wb_chunks):
        for j in range(1, n_tp // 2):
            cross.append(
                wb_copy(c, wb_ref, p, lax.rem(p + 2 * j, n_tp), wb_send.at[j, c], wb_recv.at[2 * j, c])
            )
            cross[-1].start()
    beside = [wb_copy(c, wb_ref, p, partner, wb_send.at[0, c], wb_recv.at[1, c]) for c in range(wb_chunks)]
    for copy in beside:
        copy.start()

    for copy in stat_copies:
        copy.wait_recv()
    prev_count = jnp.zeros((1, 1), jnp.float32)
    prev_sums = jnp.zeros((1, width), jnp.float32)
    for k in range(n_sp):
        block = stats[k]
        joined = (block[0:1, width : width + 1] == first) & (k < s)
        prev_count = prev_count + jnp.where(joined, block[0:1, width + 1 : width + 2], 0.0)
        prev_sums = prev_sums + jnp.where(joined, block[0:1, 0:width], 0.0)
    carried = docc.astype(jnp.float32) == first
    length = here + jnp.where(carried, prev_count, 0.0)
    running = running + jnp.where(carried, prev_sums, 0.0)
    doc_mean = running / length

    halo_copy.wait_recv()
    tpos = lax.broadcasted_iota(jnp.int32, (toks, toks + halo), 0) + halo
    spos = lax.broadcasted_iota(jnp.int32, (toks, toks + halo), 1)
    back = tpos - spos
    groups = width // group_width
    for i in range(groups):
        g = p * groups + i
        window = jnp.int32(0)
        for at, size in enumerate(pool_windows):
            window = jnp.where(g == at, size, window)
        span = jnp.minimum(length, window.astype(jnp.float32))
        band = ((back >= 0) & (back < span.astype(jnp.int32))).astype(jnp.float32).astype(jnp.bfloat16)
        cols = slice(i * group_width, (i + 1) * group_width)
        recent = dot(band, ext[:, cols])
        offset = 0.5 * (recent / span + doc_mean[:, cols]) - values[:, cols].astype(jnp.float32)
        turned = dot(offset.astype(jnp.bfloat16), wg_ref[g])
        scale = scale_ref[0:1, pl.ds(pl.multiple_of(g * group_width, group_width), group_width)]
        mixed[:, cols] = (turned * scale.astype(jnp.float32)).astype(jnp.bfloat16)

    mix_copies = []
    for k in range(1, n_tp):
        q = lax.rem(p + k, n_tp)
        mix_copies.append(
            pltpu.make_async_remote_copy(
                src_ref=mixed.at[pl.ds(pl.multiple_of(q * rows, rows), rows)], dst_ref=token_rows.at[p],
                send_sem=mix_send.at[k], recv_sem=mix_recv.at[k],
                device_id=(s, q), device_id_type=MESH,
            )
        )
        mix_copies[-1].start()
    token_rows[p] = mixed[pl.ds(pl.multiple_of(p * rows, rows), rows), :]

    onward = []
    for c in range(wb_chunks):
        for j in range(1, n_tp // 2):
            slot = lax.rem(p - 2 * j + n_tp, n_tp)
            cross[c * (n_tp // 2 - 1) + j - 1].wait_recv()
            onward.append(
                wb_copy(c, wb_all.at[slot], slot, partner, fw_send.at[j, c], wb_recv.at[2 * j + 1, c])
            )
            onward[-1].start()
    for copy in mix_copies:
        copy.wait_recv()
    own_wb.wait()
    for copy in beside + onward:
        copy.wait_recv()
    branch = alpha_mix * resid_ref[...].astype(jnp.float32)
    for k in range(n_tp):
        branch = branch + dot(token_rows[k], wb_all[k])
    out_ref[...] = layer_norm(branch, gain_ref[...]).astype(jnp.bfloat16)
    metas_ref[...] = stats[:, :, width + 128 :]
    halo_copy.wait_send()
    for copy in stat_copies + mix_copies + cross + beside + onward:
        copy.wait_send()


def expert_kernel(
    n_sp, n_tp, n_x, cap,
    normed_ref, metas_ref, eg_hbm, eu_hbm, ed_hbm, sg_hbm, su_hbm, sd_hbm, gain_ref,
    out_ref,
    eg, eu, ed, sg, su, sd, blocks, outgoing, arrived, returned, column, across, chain, acc, pick, share,
    load_sem, up_send, down_send, x_send, block_recv, go_send, go_recv, back_send, back_recv,
    across_send, across_recv, chain_send, chain_recv,
):
    n_z = n_sp // n_x
    s, p = lax.axis_index("sp"), lax.axis_index("tp")
    z, x = s // n_x, lax.rem(s, n_x)
    toks = normed_ref.shape[0]
    top = metas_ref.shape[1] // 2

    barrier = pltpu.get_barrier_semaphore()
    for k in range(1, n_sp):
        pl.semaphore_signal(barrier, inc=1, device_id=(lax.rem(s + k, n_sp), p), device_id_type=MESH)
    for k in range(1, n_tp):
        pl.semaphore_signal(barrier, inc=1, device_id=(s, lax.rem(p + k, n_tp)), device_id_type=MESH)

    loads = [
        pltpu.make_async_copy(a, b, load_sem.at[i])
        for i, (a, b) in enumerate(
            [(sg_hbm, sg), (su_hbm, su), (sd_hbm, sd), (eg_hbm.at[0], eg), (eu_hbm.at[0], eu), (ed_hbm.at[0], ed)]
        )
    ]
    for load in loads:
        load.start()
    blocks[s] = normed_ref[...]

    low = jnp.minimum(z, n_z - 1 - z)
    rising = jnp.where(z * 2 < n_z, 1, -1)
    near = [z]
    for i in range(1, n_z):
        swing = z - (i + 1) // 2 if i % 2 else z + i // 2
        near.append(jnp.where(2 * low >= i, swing, z + rising * (i - low)))

    def copy(src, dst, send, recv, where):
        return pltpu.make_async_remote_copy(
            src_ref=src, dst_ref=dst, send_sem=send, recv_sem=recv, device_id=where, device_id_type=MESH
        )

    def up(zb):
        k = zb * n_x + x
        return copy(blocks.at[k], blocks.at[k], up_send.at[zb], block_recv.at[k], (jnp.minimum(s + n_x, n_sp - 1), p))

    def down(zb):
        k = zb * n_x + x
        return copy(blocks.at[k], blocks.at[k], down_send.at[zb], block_recv.at[k], (jnp.maximum(s - n_x, 0), p))

    def beside(zb, o):
        k = zb * n_x + x
        where = (z * n_x + lax.rem(x + o, n_x), p)
        return copy(blocks.at[k], blocks.at[k], x_send.at[zb, o], block_recv.at[k], where)

    def arrival(k):
        where = (lax.rem(s + 1, n_sp), p)
        return copy(blocks.at[k], blocks.at[k], x_send.at[0, 0], block_recv.at[k], where)

    def rises(zb):
        return (zb <= z) & (z + 1 < n_z)

    def sinks(zb):
        return (zb >= z) & (z > 0)

    def relay(zb):
        @pl.when(rises(zb))
        def _():
            up(zb).start()

        @pl.when(sinks(zb))
        def _():
            down(zb).start()

        for o in range(1, n_x):
            beside(zb, o).start()

    def seat(j):
        return pl.ds(j * cap, cap)

    def go(k, j):
        return copy(
            outgoing.at[k, seat(j)], arrived.at[k, seat(j)], go_send.at[k, j], go_recv.at[k, j],
            (s, lax.rem(p + j, n_tp)),
        )

    def back(k, j):
        return copy(
            arrived.at[k, seat(j)], returned.at[k, seat(j)], back_send.at[k, j], back_recv.at[k, j],
            (s, lax.rem(p + n_tp - j, n_tp)),
        )

    def send_partial(zb, o):
        xb = lax.rem(x + o, n_x)
        k = zb * n_x + xb
        return copy(
            blocks.at[k], across.at[zb, o], across_send.at[zb, o], across_recv.at[zb, o], (z * n_x + xb, p)
        )

    def index(i, o):
        return near[i] * n_x + lax.rem(x + o, n_x)

    def dispatch(i, o):
        k = index(i, o)
        if i or o:
            arrival(k).wait_recv()
            if not o:
                relay(near[i])
        outgoing[k] = dot(pick[k], blocks[k]).astype(jnp.bfloat16)
        for j in range(1, n_tp):
            go(k, j).start()
        arrived[k, seat(0)] = outgoing[k, seat(0)]

    def experts(i, o):
        k = index(i, o)
        for j in range(1, n_tp):
            go(k, j).wait_recv()
        tokens = arrived[k]
        inner = silu_mul(dot(tokens, eg[...]), dot(tokens, eu[...]))
        arrived[k] = dot(inner, ed[...]).astype(jnp.bfloat16)
        for j in range(1, n_tp):
            back(k, j).start()
        returned[k, seat(0)] = arrived[k, seat(0)]

    def combine(i, o):
        k = index(i, o)
        for j in range(1, n_tp):
            back(k, j).wait_recv()
        both = lax.dot_general(
            share[k], returned[k], (((0,), (0,)), ((), ())), preferred_element_type=jnp.float32
        )
        partial = both[0:toks] + both[toks:]
        if o:
            blocks[k] = partial.astype(jnp.bfloat16)
            send_partial(near[i], o).start()
        else:
            column[near[i]] = partial

    pl.semaphore_wait(barrier, n_sp + n_tp - 2)
    relay(z)

    pad = -(-n_tp // 8) * 8
    expert = s * n_tp + lax.rem(p + lax.broadcasted_iota(jnp.int32, (n_sp, pad, toks), 1), n_tp)
    expert = expert.astype(jnp.float32)
    chosen = jnp.zeros((n_sp, pad, toks), jnp.float32)
    weight = jnp.zeros((n_sp, pad, toks), jnp.float32)
    for a in range(top):
        hit = metas_ref[:, a : a + 1, :] == expert
        chosen = chosen + jnp.where(hit, 1.0, 0.0)
        weight = weight + jnp.where(hit, metas_ref[:, top + a : top + a + 1, :], 0.0)
    earlier = lax.broadcasted_iota(jnp.int32, (toks, toks), 0) < lax.broadcasted_iota(jnp.int32, (toks, toks), 1)
    rank = dot(
        chosen.reshape(n_sp * pad, toks).astype(jnp.bfloat16), earlier.astype(jnp.float32).astype(jnp.bfloat16)
    ).reshape(n_sp, pad, toks)
    key = jnp.where(chosen > 0.0, rank, -1.0)
    slot = lax.broadcasted_iota(jnp.int32, (n_sp, cap, toks), 1).astype(jnp.float32)
    for j in range(n_tp):
        taken = slot == key[:, j : j + 1, :]
        pick[:, seat(j), :] = jnp.where(taken, 1.0, 0.0).astype(jnp.bfloat16)
        full = jnp.where(taken, weight[:, j : j + 1, :], 0.0)
        high = full.astype(jnp.bfloat16)
        share[:, seat(j), 0:toks] = high
        share[:, seat(j), toks:] = (full - high.astype(jnp.float32)).astype(jnp.bfloat16)

    order = [(0, 0)]
    for i in range(1, n_z):
        order += [(i, 0)] + [(i - 1, o) for o in range(1, n_x)]
    order += [(n_z - 1, o) for o in range(1, n_x)]
    for at in range(len(order) + 3):
        if at < len(order):
            dispatch(*order[at])
        if at == 0:
            for load in loads[:3]:
                load.wait()
            hidden = silu_mul(dot(normed_ref[...], sg[...]), dot(normed_ref[...], su[...]))
            acc[...] = alpha_mix * normed_ref[...].astype(jnp.float32) + dot(hidden, sd[...])
            for load in loads[3:]:
                load.wait()
        if 0 <= at - 1 < len(order):
            experts(*order[at - 1])
        if 0 <= at - 3 < len(order):
            combine(*order[at - 3])

    for zb in range(n_z):
        @pl.when(rises(zb))
        def _():
            up(zb).wait_send()

        @pl.when(sinks(zb))
        def _():
            down(zb).wait_send()

        for o in range(1, n_x):
            beside(zb, o).wait_send()

    def column_sum(zb):
        total = column[zb]
        for o in range(1, n_x):
            send_partial(zb, o).wait_recv()
            total = total + across[zb, o].astype(jnp.float32)
        column[zb] = total

    def link(side, zb):
        where = s + n_x if side == 0 else s - n_x
        where = jnp.maximum(jnp.minimum(where, n_sp - 1), 0)
        return copy(
            blocks.at[zb * n_x + x], chain.at[side, zb], chain_send.at[zb], chain_recv.at[side, zb], (where, p)
        )

    def take(side, zb, holds):
        @pl.when(holds)
        def _():
            link(side, zb).wait_recv()
            column[zb] += chain[side, zb].astype(jnp.float32)

    for i in range(n_z - 1, 0, -1):
        zb = near[i]
        column_sum(zb)
        take(0, zb, (zb > z) & (z > 0))
        take(1, zb, (zb < z) & (z + 1 < n_z))
        blocks[zb * n_x + x] = column[zb].astype(jnp.bfloat16)

        @pl.when(zb > z)
        def _():
            link(0, zb).start()

        @pl.when(zb < z)
        def _():
            link(1, zb).start()

    column_sum(z)
    take(0, z, z > 0)
    take(1, z, z + 1 < n_z)
    out_ref[...] = layer_norm(acc[...] + column[z], gain_ref[...]).astype(jnp.bfloat16)

    for i in range(1, n_z):
        link(0, near[i]).wait_send()
    for k in range(n_sp):
        for j in range(1, n_tp):
            go(k, j).wait_send()
            back(k, j).wait_send()
    for zb in range(n_z):
        for o in range(1, n_x):
            send_partial(zb, o).wait_send()


def local(
    n_sp, n_tp,
    resid, pool_in, doc_ids, w_group, pool_scale, w_branch, norm_gain, route_ids, route_wts,
    w_exp_gate, w_exp_up, w_exp_down, w_sh_gate, w_sh_up, w_sh_down, final_gain,
):
    toks, width = pool_in.shape
    rows, model = resid.shape
    depth = w_branch.shape[0]
    cap = 2 * rows * route_ids.shape[1] // (n_sp * n_tp)
    n_x = max(k for k in range(1, n_sp + 1) if n_sp % k == 0 and k * k <= n_sp)
    n_z = n_sp // n_x
    ff = w_sh_gate.shape[1]
    meta = jnp.concatenate([route_ids.astype(jnp.float32), route_wts], axis=1).T
    vmem, hbm = pl.BlockSpec(memory_space=pltpu.VMEM), pl.BlockSpec(memory_space=pl.ANY)
    dma = pltpu.SemaphoreType.DMA
    bf16, f32 = jnp.bfloat16, jnp.float32
    normed, metas = pl.pallas_call(
        functools.partial(pool_kernel, n_sp, n_tp),
        out_shape=(
            jax.ShapeDtypeStruct((rows, model), bf16),
            jax.ShapeDtypeStruct((n_sp, meta.shape[0], rows), f32),
        ),
        in_specs=[vmem] * 5 + [hbm] + [vmem] * 3,
        out_specs=(vmem, vmem),
        scratch_shapes=[
            pltpu.VMEM((halo + toks, width), bf16),
            pltpu.VMEM((n_sp, 8, width + 128 + rows), f32),
            pltpu.VMEM((toks, width), bf16),
            pltpu.VMEM((n_tp, rows, width), bf16),
            pltpu.VMEM((n_tp, depth, model), bf16),
            dma((n_sp,)), dma((n_sp,)), dma, dma, dma((n_tp,)), dma((n_tp,)),
            dma((n_tp, wb_chunks)), dma((n_tp, wb_chunks)), dma((n_tp, wb_chunks)), dma,
        ],
        compiler_params=pltpu.CompilerParams(
            collective_id=0, has_side_effects=True, vmem_limit_bytes=48 << 20
        ),
        name="pool_mixer",
    )(
        pool_in, doc_ids[:, None], doc_ids[None, :], w_group, pool_scale[None, :], w_branch,
        resid, norm_gain[None, :], meta,
    )
    seats = pltpu.VMEM((n_sp, n_tp * cap, model), bf16)
    block = (rows, model)
    return pl.pallas_call(
        functools.partial(expert_kernel, n_sp, n_tp, n_x, cap),
        out_shape=jax.ShapeDtypeStruct(block, bf16),
        in_specs=[vmem] * 2 + [hbm] * 6 + [vmem],
        out_specs=vmem,
        scratch_shapes=[
            pltpu.VMEM((model, ff), bf16), pltpu.VMEM((model, ff), bf16), pltpu.VMEM((ff, model), bf16),
            pltpu.VMEM((model, ff), bf16), pltpu.VMEM((model, ff), bf16), pltpu.VMEM((ff, model), bf16),
            pltpu.VMEM((n_sp, *block), bf16),
            seats, seats, seats,
            pltpu.VMEM((n_z, *block), f32),
            pltpu.VMEM((n_z, n_x, *block), bf16),
            pltpu.VMEM((2, n_z, *block), bf16),
            pltpu.VMEM(block, f32),
            pltpu.VMEM((n_sp, n_tp * cap, rows), bf16), pltpu.VMEM((n_sp, n_tp * cap, 2 * rows), bf16),
            dma((6,)), dma((n_z,)), dma((n_z,)), dma((n_z, n_x)), dma((n_sp,)),
            dma((n_sp, n_tp)), dma((n_sp, n_tp)), dma((n_sp, n_tp)), dma((n_sp, n_tp)),
            dma((n_z, n_x)), dma((n_z, n_x)), dma((n_z,)), dma((2, n_z)),
        ],
        compiler_params=pltpu.CompilerParams(
            collective_id=1, has_side_effects=True, vmem_limit_bytes=62 << 20
        ),
        name="routed_experts",
    )(
        normed, metas, w_exp_gate, w_exp_up, w_exp_down,
        w_sh_gate, w_sh_up, w_sh_down, final_gain[None, :],
    )


def solution(mesh):
    both = P(("sp", "tp"), None)
    stack = P(("sp", "tp"), None, None)
    placed = (
        both, P("sp", "tp"), P("sp"), P(), P(), P("tp", None), P(), both, both,
        stack, stack, stack, P(), P(), P(), P(),
    )
    return jax.shard_map(
        functools.partial(local, mesh.shape["sp"], mesh.shape["tp"]),
        mesh=mesh, in_specs=placed, out_specs=both, check_vma=False,
    )
```

profile of v0, /device:TPU:0, one launch (start us, length us, event | category | flops | bytes accessed | tf_op | source)
XLA Modules:
  0.0 203.6 jit_solution(12271960080749079182)
XLA Ops:
  0.0 0.7 convert_element_type.3
  0.7 0.7 maximum_bitcast_fusion.meta_ref
  1.4 0.7 broadcast_in_dim.17.scale_ref
  2.1 0.7 broadcast_in_dim.18.gain_ref
  2.8 1.3 broadcast_in_dim.19.gain_ref
  4.0 0.8 copy.17.docc_ref
  4.9 0.0 copy-start
  4.9 1.2 copy-done
  6.1 0.0 copy-start.2
  6.1 1.0 copy-done.2
  7.1 0.0 copy-start.3
  7.1 0.9 copy-done.3
  8.1 0.0 copy-start.4
  8.1 0.9 copy-done.4
  9.0 0.0 copy-start.6
  9.0 0.7 copy-done.6
  9.7 34.8 %pool_mixer.1 = (bf16[128,2048]{1,0:T(8,128)(2,1)S(1)}, f32[8,8,128]{2,1,0:T(8,128)S(1)}) custom-call(bf16[512,256]{1,0:T(8,128)(2,1)S(1)} %copy-done.3, s32[512,1]{1,0:T(8,128)S(1)} %copy.17.docc_ref, s32[1,512]{1,0:T(1,128)S(1)} %bitcast.5, bf16[8,128,128]{2,1,0:T(8,128)(2,1)S(1)} %copy-done.4, bf16[1,1024]{1,0:T(2,128)(2,1)S(1)} %broadcast_in_dim.17.scale_ref, ...), custom_call_target="tpu_custom_call" | custom-call | tf_op jit(solution)/shard_map/pool_mixer/pallas_call | solution.py:445
  44.6 0.0 copy-start.1
  44.6 0.8 copy-done.1
  45.4 0.0 copy-start.5
  45.4 0.6 copy-done.5
  46.0 155.8 %routed_experts.1 = bf16[128,2048]{1,0:T(8,128)(2,1)} custom-call(bf16[128,2048]{1,0:T(8,128)(2,1)} %copy-done.1, f32[8,8,128]{2,1,0:T(8,128)} %copy-done.5, bf16[1,2048,512]{2,1,0:T(8,128)(2,1)} %eg_hbm.1, bf16[1,2048,512]{2,1,0:T(8,128)(2,1)} %eu_hbm.1, bf16[1,512,2048]{2,1,0:T(8,128)(2,1)} %ed_hbm.1, bf16[2048,512]{1,0:T(8,128)(2,1)} %sg_hbm.1, ...), custom_call_target="tpu_custom_call" | custom-call | tf_op jit(solution)/shard_map/routed_experts/pallas_call | solution.py:472
  201.8 1.9 copy.19
Async XLA Ops:
  4.9 1.2 copy-start
  6.1 1.0 copy-start.2
  7.1 0.9 copy-start.3
  8.1 0.9 copy-start.4
  9.0 0.7 copy-start.6
  44.6 0.8 copy-start.1
  45.4 0.6 copy-start.5
where the time goes:
time: 204 us
  Pallas kernels  191 us (94%)
  local copies, waits for them, and re-layouts  11.6 us (6%)
    pallas_call x1, Pallas kernels, local(): pl.pallas_call(functools.partial(expert_kernel, n_sp, n_tp, n_x, cap), ou...  156 us
    pallas_call x1, Pallas kernels, local(): pl.pallas_call(functools.partial(pool_kernel, n_sp, n_tp), out_shape=(jax...  34.8 us
    unnamed x15, local copies, waits for them, and re-layouts  8.11 us

commit v1 on v0

--- a/solution.py
+++ b/solution.py
@@ -13,6 +13,7 @@
 halo = max(pool_windows)
 MESH = pl.DeviceIdType.MESH
 wb_chunks = 4
+chunks = 4
 
 
 def layer_norm(values, gain):
@@ -184,21 +185,29 @@
     n_sp, n_tp, n_x, cap,
     normed_ref, metas_ref, eg_hbm, eu_hbm, ed_hbm, sg_hbm, su_hbm, sd_hbm, gain_ref,
     out_ref,
-    eg, eu, ed, sg, su, sd, blocks, outgoing, arrived, returned, column, across, chain, acc, pick, share,
-    load_sem, up_send, down_send, x_send, block_recv, go_send, go_recv, back_send, back_recv,
-    across_send, across_recv, chain_send, chain_recv,
+    eg, eu, ed, sg, su, sd, blocks, outgoing, arrived, returned, column, partial, chain, acc, pick, share,
+    load_sem, up_send, down_send, block_recv, go_send, go_recv, back_send, back_recv,
+    chain_send, chain_recv,
 ):
     n_z = n_sp // n_x
+    peers = n_x * n_tp
     s, p = lax.axis_index("sp"), lax.axis_index("tp")
     z, x = s // n_x, lax.rem(s, n_x)
-    toks = normed_ref.shape[0]
+    toks, model = normed_ref.shape
     top = metas_ref.shape[1] // 2
+    strip = model // chunks
+
+    def mate(q):
+        return z * n_x + lax.rem(x + q // n_tp, n_x), lax.rem(p + q % n_tp, n_tp)
+
+    def home(q):
+        return z * n_x + lax.rem(x + n_x - q // n_tp, n_x), lax.rem(p + n_tp - q % n_tp, n_tp)
 
     barrier = pltpu.get_barrier_semaphore()
-    for k in range(1, n_sp):
-        pl.semaphore_signal(barrier, inc=1, device_id=(lax.rem(s + k, n_sp), p), device_id_type=MESH)
-    for k in range(1, n_tp):
-        pl.semaphore_signal(barrier, inc=1, device_id=(s, lax.rem(p + k, n_tp)), device_id_type=MESH)
+    for k in range(1, n_z):
+        pl.semaphore_signal(barrier, inc=1, device_id=(lax.rem(s + k * n_x, n_sp), p), device_id_type=MESH)
+    for q in range(1, peers):
+        pl.semaphore_signal(barrier, inc=1, device_id=mate(q), device_id_type=MESH)
 
     loads = [
         pltpu.make_async_copy(a, b, load_sem.at[i])
@@ -208,7 +217,6 @@
     ]
     for load in loads:
         load.start()
-    blocks[s] = normed_ref[...]
 
     low = jnp.minimum(z, n_z - 1 - z)
     rising = jnp.where(z * 2 < n_z, 1, -1)
@@ -222,22 +230,17 @@
             src_ref=src, dst_ref=dst, send_sem=send, recv_sem=recv, device_id=where, device_id_type=MESH
         )
 
-    def up(zb):
-        k = zb * n_x + x
-        return copy(blocks.at[k], blocks.at[k], up_send.at[zb], block_recv.at[k], (jnp.minimum(s + n_x, n_sp - 1), p))
-
-    def down(zb):
-        k = zb * n_x + x
-        return copy(blocks.at[k], blocks.at[k], down_send.at[zb], block_recv.at[k], (jnp.maximum(s - n_x, 0), p))
-
-    def beside(zb, o):
-        k = zb * n_x + x
-        where = (z * n_x + lax.rem(x + o, n_x), p)
-        return copy(blocks.at[k], blocks.at[k], x_send.at[zb, o], block_recv.at[k], where)
-
-    def arrival(k):
-        where = (lax.rem(s + 1, n_sp), p)
-        return copy(blocks.at[k], blocks.at[k], x_send.at[0, 0], block_recv.at[k], where)
+    def lane(c):
+        return pl.ds(c * strip, strip)
+
+    above = (jnp.minimum(s + n_x, n_sp - 1), p)
+    below = (jnp.maximum(s - n_x, 0), p)
+
+    def up(src, zb, c):
+        return copy(src, blocks.at[zb, :, lane(c)], up_send.at[zb, c], block_recv.at[zb, c], above)
+
+    def down(src, zb, c):
+        return copy(src, blocks.at[zb, :, lane(c)], down_send.at[zb, c], block_recv.at[zb, c], below)
 
     def rises(zb):
         return (zb <= z) & (z + 1 < n_z)
@@ -245,185 +248,172 @@
     def sinks(zb):
         return (zb >= z) & (z > 0)
 
-    def relay(zb):
+    def relay(zb, c):
+        src = blocks.at[zb, :, lane(c)]
+
         @pl.when(rises(zb))
         def _():
-            up(zb).start()
+            up(src, zb, c).start()
 
         @pl.when(sinks(zb))
         def _():
-            down(zb).start()
-
-        for o in range(1, n_x):
-            beside(zb, o).start()
-
-    def seat(j):
-        return pl.ds(j * cap, cap)
-
-    def go(k, j):
+            down(src, zb, c).start()
+
+    def receive(i):
+        for c in range(chunks):
+            up(blocks.at[near[i], :, lane(c)], near[i], c).wait_recv()
+            relay(near[i], c)
+
+    def seat(q):
+        return pl.ds(q * cap, cap)
+
+    def go(i, q):
         return copy(
-            outgoing.at[k, seat(j)], arrived.at[k, seat(j)], go_send.at[k, j], go_recv.at[k, j],
-            (s, lax.rem(p + j, n_tp)),
-        )
-
-    def back(k, j):
+            outgoing.at[i, seat(q)], arrived.at[i, seat(q)], go_send.at[i, q], go_recv.at[i, q], mate(q)
+        )
+
+    def back(i, q):
         return copy(
-            arrived.at[k, seat(j)], returned.at[k, seat(j)], back_send.at[k, j], back_recv.at[k, j],
-            (s, lax.rem(p + n_tp - j, n_tp)),
-        )
-
-    def send_partial(zb, o):
-        xb = lax.rem(x + o, n_x)
-        k = zb * n_x + xb
+            arrived.at[i, seat(q)], returned.at[i, seat(q)], back_send.at[i, q], back_recv.at[i, q], home(q)
+        )
+
+    far_first = sorted(range(1, peers), key=lambda q: (q // n_tp == 0) + (q % n_tp == 0))
+
+    def dispatch(i):
+        outgoing[i] = dot(pick[near[i]], blocks[near[i]]).astype(jnp.bfloat16)
+        for q in far_first:
+            go(i, q).start()
+        arrived[i, seat(0)] = outgoing[i, seat(0)]
+
+    def experts(i):
+        for q in range(1, peers):
+            go(i, q).wait_recv()
+        tokens = arrived[i]
+        inner = silu_mul(dot(tokens, eg[...]), dot(tokens, eu[...]))
+        arrived[i] = dot(inner, ed[...]).astype(jnp.bfloat16)
+        for q in far_first:
+            back(i, q).start()
+        returned[i, seat(0)] = arrived[i, seat(0)]
+
+    def combine(i):
+        for q in range(1, peers):
+            back(i, q).wait_recv()
+        both = lax.dot_general(
+            share[near[i]], returned[i], (((0,), (0,)), ((), ())), preferred_element_type=jnp.float32
+        )
+        total = both[0:toks] + both[toks:]
+        column[near[i]] = total if i else total + acc[...]
+
+    def link(side, zb, c):
         return copy(
-            blocks.at[k], across.at[zb, o], across_send.at[zb, o], across_recv.at[zb, o], (z * n_x + xb, p)
-        )
-
-    def index(i, o):
-        return near[i] * n_x + lax.rem(x + o, n_x)
-
-    def dispatch(i, o):
-        k = index(i, o)
-        if i or o:
-            arrival(k).wait_recv()
-            if not o:
-                relay(near[i])
-        outgoing[k] = dot(pick[k], blocks[k]).astype(jnp.bfloat16)
-        for j in range(1, n_tp):
-            go(k, j).start()
-        arrived[k, seat(0)] = outgoing[k, seat(0)]
-
-    def experts(i, o):
-        k = index(i, o)
-        for j in range(1, n_tp):
-            go(k, j).wait_recv()
-        tokens = arrived[k]
-        inner = silu_mul(dot(tokens, eg[...]), dot(tokens, eu[...]))
-        arrived[k] = dot(inner, ed[...]).astype(jnp.bfloat16)
-        for j in range(1, n_tp):
-            back(k, j).start()
-        returned[k, seat(0)] = arrived[k, seat(0)]
-
-    def combine(i, o):
-        k = index(i, o)
-        for j in range(1, n_tp):
-            back(k, j).wait_recv()
-        both = lax.dot_general(
-            share[k], returned[k], (((0,), (0,)), ((), ())), preferred_element_type=jnp.float32
-        )
-        partial = both[0:toks] + both[toks:]
-        if o:
-            blocks[k] = partial.astype(jnp.bfloat16)
-            send_partial(near[i], o).start()
-        else:
-            column[near[i]] = partial
-
-    pl.semaphore_wait(barrier, n_sp + n_tp - 2)
-    relay(z)
-
-    pad = -(-n_tp // 8) * 8
-    expert = s * n_tp + lax.rem(p + lax.broadcasted_iota(jnp.int32, (n_sp, pad, toks), 1), n_tp)
-    expert = expert.astype(jnp.float32)
-    chosen = jnp.zeros((n_sp, pad, toks), jnp.float32)
-    weight = jnp.zeros((n_sp, pad, toks), jnp.float32)
-    for a in range(top):
-        hit = metas_ref[:, a : a + 1, :] == expert
-        chosen = chosen + jnp.where(hit, 1.0, 0.0)
-        weight = weight + jnp.where(hit, metas_ref[:, top + a : top + a + 1, :], 0.0)
-    earlier = lax.broadcasted_iota(jnp.int32, (toks, toks), 0) < lax.broadcasted_iota(jnp.int32, (toks, toks), 1)
-    rank = dot(
-        chosen.reshape(n_sp * pad, toks).astype(jnp.bfloat16), earlier.astype(jnp.float32).astype(jnp.bfloat16)
-    ).reshape(n_sp, pad, toks)
-    key = jnp.where(chosen > 0.0, rank, -1.0)
-    slot = lax.broadcasted_iota(jnp.int32, (n_sp, cap, toks), 1).astype(jnp.float32)
-    for j in range(n_tp):
-        taken = slot == key[:, j : j + 1, :]
-        pick[:, seat(j), :] = jnp.where(taken, 1.0, 0.0).astype(jnp.bfloat16)
-        full = jnp.where(taken, weight[:, j : j + 1, :], 0.0)
-        high = full.astype(jnp.bfloat16)
-        share[:, seat(j), 0:toks] = high
-        share[:, seat(j), toks:] = (full - high.astype(jnp.float32)).astype(jnp.bfloat16)
-
-    order = [(0, 0)]
-    for i in range(1, n_z):
-        order += [(i, 0)] + [(i - 1, o) for o in range(1, n_x)]
-    order += [(n_z - 1, o) for o in range(1, n_x)]
-    for at in range(len(order) + 3):
-        if at < len(order):
-            dispatch(*order[at])
-        if at == 0:
-            for load in loads[:3]:
-                load.wait()
-            hidden = silu_mul(dot(normed_ref[...], sg[...]), dot(normed_ref[...], su[...]))
-            acc[...] = alpha_mix * normed_ref[...].astype(jnp.float32) + dot(hidden, sd[...])
-            for load in loads[3:]:
-                load.wait()
-        if 0 <= at - 1 < len(order):
-            experts(*order[at - 1])
-        if 0 <= at - 3 < len(order):
-            combine(*order[at - 3])
-
-    for zb in range(n_z):
-        @pl.when(rises(zb))
-        def _():
-            up(zb).wait_send()
-
-        @pl.when(sinks(zb))
-        def _():
-            down(zb).wait_send()
-
-        for o in range(1, n_x):
-            beside(zb, o).wait_send()
-
-    def column_sum(zb):
-        total = column[zb]
-        for o in range(1, n_x):
-            send_partial(zb, o).wait_recv()
-            total = total + across[zb, o].astype(jnp.float32)
-        column[zb] = total
-
-    def link(side, zb):
-        where = s + n_x if side == 0 else s - n_x
-        where = jnp.maximum(jnp.minimum(where, n_sp - 1), 0)
-        return copy(
-            blocks.at[zb * n_x + x], chain.at[side, zb], chain_send.at[zb], chain_recv.at[side, zb], (where, p)
-        )
-
-    def take(side, zb, holds):
+            partial.at[zb, :, lane(c)], chain.at[side, zb, :, lane(c)], chain_send.at[zb, c],
+            chain_recv.at[side, zb, c], above if side == 0 else below,
+        )
+
+    def take(side, zb, c, holds):
         @pl.when(holds)
         def _():
-            link(side, zb).wait_recv()
-            column[zb] += chain[side, zb].astype(jnp.float32)
-
-    for i in range(n_z - 1, 0, -1):
+            link(side, zb, c).wait_recv()
+            column[zb, :, lane(c)] += chain[side, zb, :, lane(c)].astype(jnp.float32)
+
+    def pass_on(i):
         zb = near[i]
-        column_sum(zb)
-        take(0, zb, (zb > z) & (z > 0))
-        take(1, zb, (zb < z) & (z + 1 < n_z))
-        blocks[zb * n_x + x] = column[zb].astype(jnp.bfloat16)
-
-        @pl.when(zb > z)
-        def _():
-            link(0, zb).start()
-
-        @pl.when(zb < z)
-        def _():
-            link(1, zb).start()
-
-    column_sum(z)
-    take(0, z, z > 0)
-    take(1, z, z + 1 < n_z)
-    out_ref[...] = layer_norm(acc[...] + column[z], gain_ref[...]).astype(jnp.bfloat16)
-
+        for c in range(chunks):
+            take(0, zb, c, (zb > z) & (z > 0))
+            take(1, zb, c, (zb < z) & (z + 1 < n_z))
+            partial[zb, :, lane(c)] = column[zb, :, lane(c)].astype(jnp.bfloat16)
+
+            @pl.when(zb > z)
+            def _():
+                link(0, zb, c).start()
+
+            @pl.when(zb < z)
+            def _():
+                link(1, zb, c).start()
+
+    def shared():
+        for load in loads[:3]:
+            load.wait()
+        hidden = silu_mul(dot(normed_ref[...], sg[...]), dot(normed_ref[...], su[...]))
+        acc[...] = alpha_mix * normed_ref[...].astype(jnp.float32) + dot(hidden, sd[...])
+        for load in loads[3:]:
+            load.wait()
+
+    blocks[z] = normed_ref[...]
+    pl.semaphore_wait(barrier, n_z + peers - 2)
+    for c in range(chunks):
+        relay(z, c)
+
+    expert_at = [z * n_x * n_tp + lax.rem(x + q // n_tp, n_x) * n_tp + lax.rem(p + q % n_tp, n_tp) for q in range(peers)]
+    earlier = lax.broadcasted_iota(jnp.int32, (toks, toks), 0) < lax.broadcasted_iota(jnp.int32, (toks, toks), 1)
+    earlier = earlier.astype(jnp.float32).astype(jnp.bfloat16)
+    row = lax.broadcasted_iota(jnp.int32, (peers, toks), 0)
+    expert = jnp.zeros((peers, toks), jnp.int32)
+    for q in range(peers):
+        expert = jnp.where(row == q, expert_at[q], expert)
+    expert = expert.astype(jnp.float32)
+    slot = lax.broadcasted_iota(jnp.int32, (cap, toks), 0).astype(jnp.float32)
+
+    def plan(i):
+        zb = near[i]
+        meta = metas_ref[zb * n_x + x]
+        chosen = jnp.zeros((peers, toks), jnp.float32)
+        weight = jnp.zeros((peers, toks), jnp.float32)
+        for a in range(top):
+            hit = meta[a : a + 1, :] == expert
+            chosen = chosen + jnp.where(hit, 1.0, 0.0)
+            weight = weight + jnp.where(hit, meta[top + a : top + a + 1, :], 0.0)
+        key = jnp.where(chosen > 0.0, dot(chosen.astype(jnp.bfloat16), earlier), -1.0)
+        for q in range(peers):
+            taken = slot == key[q : q + 1, :]
+            pick[zb, seat(q), :] = jnp.where(taken, 1.0, 0.0).astype(jnp.bfloat16)
+            full = jnp.where(taken, weight[q : q + 1, :], 0.0)
+            high = full.astype(jnp.bfloat16)
+            share[zb, seat(q), 0:toks] = high
+            share[zb, seat(q), toks:] = (full - high.astype(jnp.float32)).astype(jnp.bfloat16)
+
+    plan(0)
+    dispatch(0)
     for i in range(1, n_z):
-        link(0, near[i]).wait_send()
-    for k in range(n_sp):
-        for j in range(1, n_tp):
-            go(k, j).wait_send()
-            back(k, j).wait_send()
+        plan(i)
+    shared()
+    for i in range(1, n_z):
+        receive(i)
+        dispatch(i)
+    last = n_z - 1
+    for i in range(last, 0, -1):
+        experts(i)
+    combine(last)
+    pass_on(last)
+    experts(0)
+    for i in range(last - 1, 0, -1):
+        combine(i)
+        pass_on(i)
+    combine(0)
+    for c in range(chunks):
+        take(0, z, c, z > 0)
+        take(1, z, c, z + 1 < n_z)
+    out_ref[...] = layer_norm(column[z], gain_ref[...]).astype(jnp.bfloat16)
+
     for zb in range(n_z):
-        for o in range(1, n_x):
-            send_partial(zb, o).wait_send()
+        for c in range(chunks):
+            src = blocks.at[zb, :, lane(c)]
+
+            @pl.when(rises(zb))
+            def _():
+                up(src, zb, c).wait_send()
+
+            @pl.when(sinks(zb))
+            def _():
+                down(src, zb, c).wait_send()
+
+    for i in range(1, n_z):
+        for c in range(chunks):
+            link(0, near[i], c).wait_send()
+    for i in range(n_z):
+        for q in range(1, peers):
+            go(i, q).wait_send()
+            back(i, q).wait_send()
 
 
 def local(
@@ -467,7 +457,8 @@
         pool_in, doc_ids[:, None], doc_ids[None, :], w_group, pool_scale[None, :], w_branch,
         resid, norm_gain[None, :], meta,
     )
-    seats = pltpu.VMEM((n_sp, n_tp * cap, model), bf16)
+    peers = n_x * n_tp
+    seats = pltpu.VMEM((n_z, peers * cap, model), bf16)
     block = (rows, model)
     return pl.pallas_call(
         functools.partial(expert_kernel, n_sp, n_tp, n_x, cap),
@@ -477,16 +468,16 @@
         scratch_shapes=[
             pltpu.VMEM((model, ff), bf16), pltpu.VMEM((model, ff), bf16), pltpu.VMEM((ff, model), bf16),
             pltpu.VMEM((model, ff), bf16), pltpu.VMEM((model, ff), bf16), pltpu.VMEM((ff, model), bf16),
-            pltpu.VMEM((n_sp, *block), bf16),
+            pltpu.VMEM((n_z, *block), bf16),
             seats, seats, seats,
             pltpu.VMEM((n_z, *block), f32),
-            pltpu.VMEM((n_z, n_x, *block), bf16),
+            pltpu.VMEM((n_z, *block), bf16),
             pltpu.VMEM((2, n_z, *block), bf16),
             pltpu.VMEM(block, f32),
-            pltpu.VMEM((n_sp, n_tp * cap, rows), bf16), pltpu.VMEM((n_sp, n_tp * cap, 2 * rows), bf16),
-            dma((6,)), dma((n_z,)), dma((n_z,)), dma((n_z, n_x)), dma((n_sp,)),
-            dma((n_sp, n_tp)), dma((n_sp, n_tp)), dma((n_sp, n_tp)), dma((n_sp, n_tp)),
-            dma((n_z, n_x)), dma((n_z, n_x)), dma((n_z,)), dma((2, n_z)),
+            pltpu.VMEM((n_z, peers * cap, rows), bf16), pltpu.VMEM((n_z, peers * cap, 2 * rows), bf16),
+            dma((6,)), dma((n_z, chunks)), dma((n_z, chunks)), dma((n_z, chunks)),
+            dma((n_z, peers)), dma((n_z, peers)), dma((n_z, peers)), dma((n_z, peers)),
+            dma((n_z, chunks)), dma((2, n_z, chunks)),
         ],
         compiler_params=pltpu.CompilerParams(
             collective_id=1, has_side_effects=True, vmem_limit_bytes=62 << 20

time: 204 us -> 156 us (0.76)
  Pallas kernels: 191 us -> 143 us
    pallas_call x1, Pallas kernels: 156 us -> 108 us  [local(): pl.pallas_call(functools.partial(expert_kernel, n_sp, n_tp, n_x, cap), ou...]
where the time goes in v1:
time: 156 us
  Pallas kernels  143 us (92%)
  local copies, waits for them, and re-layouts  11.6 us (7%)
    pallas_call x1, Pallas kernels, local(): pl.pallas_call(functools.partial(expert_kernel, n_sp, n_tp, n_x, cap), ou...  108 us
    pallas_call x1, Pallas kernels, local(): pl.pallas_call(functools.partial(pool_kernel, n_sp, n_tp), out_shape=(jax...  34.8 us
    unnamed x15, local copies, waits for them, and re-layouts  8.11 us

profile of v1, /device:TPU:0, one launch (start us, length us, event | category | flops | bytes accessed | tf_op | source)
XLA Modules:
  0.0 155.8 jit_solution(9606449510217096893)
XLA Ops:
  0.0 0.7 convert_element_type.3
  0.7 0.7 maximum_bitcast_fusion.meta_ref
  1.4 0.7 broadcast_in_dim.17.scale_ref
  2.1 0.7 broadcast_in_dim.18.gain_ref
  2.8 1.3 broadcast_in_dim.19.gain_ref
  4.0 0.8 copy.17.docc_ref
  4.9 0.0 copy-start
  4.9 1.2 copy-done
  6.1 0.0 copy-start.2
  6.1 1.0 copy-done.2
  7.1 0.0 copy-start.3
  7.1 0.9 copy-done.3
  8.1 0.0 copy-start.4
  8.1 0.9 copy-done.4
  9.0 0.0 copy-start.6
  9.0 0.7 copy-done.6
  9.7 34.8 %pool_mixer.1 = (bf16[128,2048]{1,0:T(8,128)(2,1)S(1)}, f32[8,8,128]{2,1,0:T(8,128)S(1)}) custom-call(bf16[512,256]{1,0:T(8,128)(2,1)S(1)} %copy-done.3, s32[512,1]{1,0:T(8,128)S(1)} %copy.17.docc_ref, s32[1,512]{1,0:T(1,128)S(1)} %bitcast.5, bf16[8,128,128]{2,1,0:T(8,128)(2,1)S(1)} %copy-done.4, bf16[1,1024]{1,0:T(2,128)(2,1)S(1)} %broadcast_in_dim.17.scale_ref, ...), custom_call_target="tpu_custom_call" | custom-call | tf_op jit(solution)/shard_map/pool_mixer/pallas_call | solution.py:435
  44.6 0.0 copy-start.1
  44.6 0.8 copy-done.1
  45.4 0.0 copy-start.5
  45.4 0.6 copy-done.5
  46.0 108.0 %routed_experts.1 = bf16[128,2048]{1,0:T(8,128)(2,1)} custom-call(bf16[128,2048]{1,0:T(8,128)(2,1)} %copy-done.1, f32[8,8,128]{2,1,0:T(8,128)} %copy-done.5, bf16[1,2048,512]{2,1,0:T(8,128)(2,1)} %eg_hbm.1, bf16[1,2048,512]{2,1,0:T(8,128)(2,1)} %eu_hbm.1, bf16[1,512,2048]{2,1,0:T(8,128)(2,1)} %ed_hbm.1, bf16[2048,512]{1,0:T(8,128)(2,1)} %sg_hbm.1, ...), custom_call_target="tpu_custom_call" | custom-call | tf_op jit(solution)/shard_map/routed_experts/pallas_call | solution.py:463
  153.9 1.9 %copy.19 = bf16[128,2048]{1,0:T(8,128)(2,1)} copy(bf16[128,2048]{1,0:T(8,128)(2,1)} %routed_experts.1) | data formatting | bytes 1048576
Async XLA Ops:
  4.9 1.2 copy-start
  6.1 1.0 copy-start.2
  7.1 0.9 copy-start.3
  8.1 0.9 copy-start.4
  9.0 0.7 copy-start.6
  44.6 0.8 copy-start.1
  45.4 0.6 copy-start.5

commit v2 on v1

v2 whole, which is shorter than its diff:
```python
import functools

import jax
import jax.numpy as jnp
from jax import lax
from jax.experimental import pallas as pl
from jax.experimental.pallas import tpu as pltpu
from jax.sharding import PartitionSpec as P

pool_windows = (2, 4, 8, 16, 16, 32, 64, 128)
alpha_mix = 8.0**0.25
norm_eps = 1e-05
halo = max(pool_windows)
MESH = pl.DeviceIdType.MESH
wb_cuts = 4
chunks = 4


def layer_norm(values, gain):
    center = values - jnp.mean(values, axis=-1, keepdims=True)
    spread = jnp.mean(center * center, axis=-1, keepdims=True)
    return center * lax.rsqrt(spread + norm_eps) * gain.astype(jnp.float32)


def dot(a, b):
    return jnp.dot(a, b, preferred_element_type=jnp.float32)


def silu_mul(gate, up):
    return (gate / (1.0 + jnp.exp(-gate)) * up).astype(jnp.bfloat16)


def layer_kernel(
    n_sp, n_tp, n_x, cap, top,
    pool_hbm, doc_hbm, wg_hbm, scale_hbm, wb_hbm, resid_hbm, ngain_hbm, ids_hbm, wts_hbm,
    eg_hbm, eu_hbm, ed_hbm, sg_hbm, su_hbm, sd_hbm, fgain_hbm,
    out_ref,
    ext, doc, wg, scales, flat, resid, ngain, ids, wts, fgain,
    stats, mixed, token_rows, wb_all,
    eg, eu, ed, sg, su, sd, blocks, outgoing, arrived, returned, column, partial, chain, acc, pick, share,
    in_sem, stat_send, stat_recv, halo_send, halo_recv, mix_send, mix_recv,
    wby_send, wby_recv, wbx_send, wbx_recv, side_send, side_recv, fw_send, fw_recv,
    load_sem, up_send, down_send, block_recv, go_send, go_recv, back_send, back_recv,
    chain_send, chain_recv,
):
    n_z = n_sp // n_x
    peers = n_x * n_tp
    s, p = lax.axis_index("sp"), lax.axis_index("tp")
    z, x = s // n_x, lax.rem(s, n_x)
    toks, width = mixed.shape
    group_width = wg.shape[1]
    rows, model = resid.shape
    depth = wb_all.shape[1]
    partner = p + 1 - 2 * lax.rem(p, 2)
    strip = model // chunks
    piece = depth // n_x
    cuts = max(1, min(wb_cuts, piece // 32))
    cut = piece // cuts

    def mate(q):
        return z * n_x + lax.rem(x + q // n_tp, n_x), lax.rem(p + q % n_tp, n_tp)

    def home(q):
        return z * n_x + lax.rem(x + n_x - q // n_tp, n_x), lax.rem(p + n_tp - q % n_tp, n_tp)

    barrier = pltpu.get_barrier_semaphore()
    for k in range(1, n_sp):
        pl.semaphore_signal(barrier, inc=1, device_id=(lax.rem(s + k, n_sp), p), device_id_type=MESH)
    for q in range(1, peers):
        if q % n_tp:
            pl.semaphore_signal(barrier, inc=1, device_id=mate(q), device_id_type=MESH)

    inputs = [
        pltpu.make_async_copy(a, b, in_sem.at[i])
        for i, (a, b) in enumerate(
            [
                (wb_hbm, wb_all.at[p]), (pool_hbm, ext.at[pl.ds(halo, toks)]), (doc_hbm, doc), (ids_hbm, ids),
                (wts_hbm, wts), (wg_hbm, wg), (scale_hbm, scales), (resid_hbm, resid), (ngain_hbm, ngain),
                (fgain_hbm, fgain),
            ]
        )
    ]
    for load in inputs:
        load.start()
    loads = [
        pltpu.make_async_copy(a, b, load_sem.at[i])
        for i, (a, b) in enumerate(
            [(sg_hbm, sg), (su_hbm, su), (sd_hbm, sd), (eg_hbm.at[0], eg), (eu_hbm.at[0], eu), (ed_hbm.at[0], ed)]
        )
    ]

    low = jnp.minimum(z, n_z - 1 - z)
    rising = jnp.where(z * 2 < n_z, 1, -1)
    near = [z]
    for i in range(1, n_z):
        swing = z - (i + 1) // 2 if i % 2 else z + i // 2
        near.append(jnp.where(2 * low >= i, swing, z + rising * (i - low)))

    def copy(src, dst, send, recv, where):
        return pltpu.make_async_remote_copy(
            src_ref=src, dst_ref=dst, send_sem=send, recv_sem=recv, device_id=where, device_id_type=MESH
        )

    def lane(c):
        return pl.ds(c * strip, strip)

    above = (jnp.minimum(s + n_x, n_sp - 1), p)
    below = (jnp.maximum(s - n_x, 0), p)

    def up(src, zb, c):
        return copy(src, blocks.at[zb, :, lane(c)], up_send.at[zb, c], block_recv.at[zb, c], above)

    def down(src, zb, c):
        return copy(src, blocks.at[zb, :, lane(c)], down_send.at[zb, c], block_recv.at[zb, c], below)

    def rises(zb):
        return (zb <= z) & (z + 1 < n_z)

    def sinks(zb):
        return (zb >= z) & (z > 0)

    def relay(zb, c):
        src = blocks.at[zb, :, lane(c)]

        @pl.when(rises(zb))
        def _():
            up(src, zb, c).start()

        @pl.when(sinks(zb))
        def _():
            down(src, zb, c).start()

    def receive(i):
        for c in range(chunks):
            up(blocks.at[near[i], :, lane(c)], near[i], c).wait_recv()
            relay(near[i], c)

    def seat(q):
        return pl.ds(q * cap, cap)

    def go(i, q):
        return copy(
            outgoing.at[i, seat(q)], arrived.at[i, seat(q)], go_send.at[i, q], go_recv.at[i, q], mate(q)
        )

    def back(i, q):
        return copy(
            arrived.at[i, seat(q)], returned.at[i, seat(q)], back_send.at[i, q], back_recv.at[i, q], home(q)
        )

    far_first = sorted(range(1, peers), key=lambda q: (q // n_tp == 0) + (q % n_tp == 0))

    def dispatch(i):
        outgoing[i] = dot(pick[near[i]], blocks[near[i]]).astype(jnp.bfloat16)
        for q in far_first:
            go(i, q).start()
        arrived[i, seat(0)] = outgoing[i, seat(0)]

    def experts(i):
        for q in range(1, peers):
            go(i, q).wait_recv()
        tokens = arrived[i]
        inner = silu_mul(dot(tokens, eg[...]), dot(tokens, eu[...]))
        arrived[i] = dot(inner, ed[...]).astype(jnp.bfloat16)
        for q in far_first:
            back(i, q).start()
        returned[i, seat(0)] = arrived[i, seat(0)]

    def combine(i):
        for q in range(1, peers):
            back(i, q).wait_recv()
        both = lax.dot_general(
            share[near[i]], returned[i], (((0,), (0,)), ((), ())), preferred_element_type=jnp.float32
        )
        total = both[0:rows] + both[rows:]
        column[near[i]] = total if i else total + acc[...]

    def link(side, zb, c):
        return copy(
            partial.at[zb, :, lane(c)], chain.at[side, zb, :, lane(c)], chain_send.at[zb, c],
            chain_recv.at[side, zb, c], above if side == 0 else below,
        )

    def take(side, zb, c, holds):
        @pl.when(holds)
        def _():
            link(side, zb, c).wait_recv()
            column[zb, :, lane(c)] += chain[side, zb, :, lane(c)].astype(jnp.float32)

    def pass_on(i):
        zb = near[i]
        for c in range(chunks):
            take(0, zb, c, (zb > z) & (z > 0))
            take(1, zb, c, (zb < z) & (z + 1 < n_z))
            partial[zb, :, lane(c)] = column[zb, :, lane(c)].astype(jnp.bfloat16)

            @pl.when(zb > z)
            def _():
                link(0, zb, c).start()

            @pl.when(zb < z)
            def _():
                link(1, zb, c).start()

    def shared():
        for load in loads[:3]:
            load.wait()
        hidden = silu_mul(dot(blocks[z], sg[...]), dot(blocks[z], su[...]))
        acc[...] = alpha_mix * blocks[z].astype(jnp.float32) + dot(hidden, sd[...])
        for load in loads[3:]:
            load.wait()


    def wb_rows(at, c):
        return pl.ds(pl.multiple_of(at * piece + c * cut, cut), cut)

    def wb_copy(slot, at, c, send, recv, where):
        src = wb_all.at[slot, wb_rows(at, c)]
        return copy(src, src, send, recv, where)

    def across(j, c):
        return wb_copy(p, x, c, wby_send.at[j, c], wby_recv.at[j, c], (s, lax.rem(p + 2 * j, n_tp)))

    def slot_of(j):
        return lax.rem(p - 2 * j + n_tp, n_tp)

    def along(j, o, c):
        where = (z * n_x + lax.rem(x + o, n_x), p)
        return wb_copy(slot_of(j), x, c, wbx_send.at[j, o, c], wbx_recv.at[j, o, c], where)

    def onward(j, o, c):
        at = lax.rem(x + n_x - o, n_x)
        return wb_copy(slot_of(j), at, c, fw_send.at[j, o, c], fw_recv.at[j, o, c], (s, partner))

    steps = range(1, n_tp // 2)

    def spread(c):
        for j in steps:
            across(j, c).wait_recv()
            for o in range(1, n_x):
                along(j, o, c).start()
            onward(j, 0, c).start()

    def gather(c):
        for j in steps:
            for o in range(1, n_x):
                along(j, o, c).wait_recv()
                onward(j, o, c).start()

    side = copy(wb_all.at[p], wb_all.at[p], side_send, side_recv, (s, partner))
    halo_copy = copy(
        ext.at[pl.ds(toks, halo)], ext.at[pl.ds(0, halo)], halo_send, halo_recv, (lax.rem(s + 1, n_sp), p)
    )
    stat_copies = [
        copy(stats.at[s], stats.at[s], stat_send.at[k], stat_recv.at[k], (lax.rem(s + k, n_sp), p))
        for k in range(1, n_sp)
    ]
    inputs[0].wait()
    pl.semaphore_wait(barrier, n_sp - 1 + n_x * (n_tp - 1))
    for c in range(cuts):
        for j in steps:
            across(j, c).start()
    side.start()
    for load in inputs[1:5]:
        load.wait()
    halo_copy.start()

    values = ext[halo:, :]
    docr = doc[...][None, :]
    docc = jnp.transpose(jnp.broadcast_to(docr.astype(jnp.float32), (128, toks)))[:, 0:1]
    docr = docr.astype(jnp.float32)
    last = jnp.max(docr, axis=1, keepdims=True)
    first = jnp.min(docr, axis=1, keepdims=True)
    tail = (docr == last).astype(jnp.float32)
    tail_count = jnp.sum(tail, axis=1, keepdims=True)
    sums = dot(jnp.broadcast_to(tail, (8, toks)).astype(jnp.bfloat16), values)
    lane_at = lax.broadcasted_iota(jnp.int32, (8, 128), 1)
    stats[s, :, 0:width] = sums
    stats[s, 0:top, width + 128 :] = ids[...].astype(jnp.float32)
    stats[s, top : 2 * top, width + 128 :] = wts[...]
    stats[s, :, width : width + 128] = jnp.where(lane_at == 0, last, tail_count)
    for each in stat_copies:
        each.start()
    for load in loads:
        load.start()

    tpos = lax.broadcasted_iota(jnp.int32, (toks, toks), 0)
    spos = lax.broadcasted_iota(jnp.int32, (toks, toks), 1)
    same = ((docc == docr) & (spos <= tpos)).astype(jnp.float32)
    here = jnp.sum(same, axis=1, keepdims=True)
    running = dot(same.astype(jnp.bfloat16), values)
    spread(0)

    for each in stat_copies:
        each.wait_recv()
    prev_count = jnp.zeros((1, 1), jnp.float32)
    prev_sums = jnp.zeros((1, width), jnp.float32)
    for k in range(n_sp):
        block = stats[k]
        joined = (block[0:1, width : width + 1] == first) & (k < s)
        prev_count = prev_count + jnp.where(joined, block[0:1, width + 1 : width + 2], 0.0)
        prev_sums = prev_sums + jnp.where(joined, block[0:1, 0:width], 0.0)
    carried = docc == first
    length = here + jnp.where(carried, prev_count, 0.0)
    running = running + jnp.where(carried, prev_sums, 0.0)
    doc_mean = running / length

    halo_copy.wait_recv()
    for load in inputs[5:]:
        load.wait()
    if cuts > 1:
        spread(1)
    tpos = lax.broadcasted_iota(jnp.int32, (toks, toks + halo), 0) + halo
    spos = lax.broadcasted_iota(jnp.int32, (toks, toks + halo), 1)
    away = tpos - spos
    groups = width // group_width
    flat[...] = scales[...].astype(jnp.float32)[None, :]
    for i in range(groups):
        g = p * groups + i
        window = jnp.int32(0)
        for at, size in enumerate(pool_windows):
            window = jnp.where(g == at, size, window)
        span = jnp.minimum(length, window.astype(jnp.float32))
        band = ((away >= 0) & (away < span.astype(jnp.int32))).astype(jnp.float32).astype(jnp.bfloat16)
        cols = slice(i * group_width, (i + 1) * group_width)
        recent = dot(band, ext[:, cols])
        offset = 0.5 * (recent / span + doc_mean[:, cols]) - values[:, cols].astype(jnp.float32)
        turned = dot(offset.astype(jnp.bfloat16), wg[g])
        scale = flat[0:1, pl.ds(pl.multiple_of(g * group_width, group_width), group_width)]
        mixed[:, cols] = (turned * scale).astype(jnp.bfloat16)

    mix_copies = []
    for k in range(1, n_tp):
        q = lax.rem(p + k, n_tp)
        mix_copies.append(
            copy(
                mixed.at[pl.ds(pl.multiple_of(q * rows, rows), rows)], token_rows.at[p],
                mix_send.at[k], mix_recv.at[k], (s, q),
            )
        )
        mix_copies[-1].start()
    token_rows[p] = mixed[pl.ds(pl.multiple_of(p * rows, rows), rows), :]
    for c in range(2, cuts):
        spread(c)
        gather(c - 2)

    expert_at = [z * n_x * n_tp + lax.rem(x + q // n_tp, n_x) * n_tp + lax.rem(p + q % n_tp, n_tp) for q in range(peers)]
    earlier = lax.broadcasted_iota(jnp.int32, (rows, rows), 0) < lax.broadcasted_iota(jnp.int32, (rows, rows), 1)
    earlier = earlier.astype(jnp.float32).astype(jnp.bfloat16)
    row = lax.broadcasted_iota(jnp.int32, (peers, rows), 0)
    expert = jnp.zeros((peers, rows), jnp.int32)
    for q in range(peers):
        expert = jnp.where(row == q, expert_at[q], expert)
    expert = expert.astype(jnp.float32)
    slot = lax.broadcasted_iota(jnp.int32, (cap, rows), 0).astype(jnp.float32)

    def plan(i):
        zb = near[i]
        meta = stats[zb * n_x + x, :, width + 128 :]
        chosen = jnp.zeros((peers, rows), jnp.float32)
        weight = jnp.zeros((peers, rows), jnp.float32)
        for a in range(top):
            hit = meta[a : a + 1, :] == expert
            chosen = chosen + jnp.where(hit, 1.0, 0.0)
            weight = weight + jnp.where(hit, meta[top + a : top + a + 1, :], 0.0)
        key = jnp.where(chosen > 0.0, dot(chosen.astype(jnp.bfloat16), earlier), -1.0)
        for q in range(peers):
            taken = slot == key[q : q + 1, :]
            pick[zb, seat(q), :] = jnp.where(taken, 1.0, 0.0).astype(jnp.bfloat16)
            full = jnp.where(taken, weight[q : q + 1, :], 0.0)
            high = full.astype(jnp.bfloat16)
            share[zb, seat(q), 0:rows] = high
            share[zb, seat(q), rows:] = (full - high.astype(jnp.float32)).astype(jnp.bfloat16)

    plan(0)
    if cuts > 1:
        gather(cuts - 2)
    for i in range(1, n_z):
        plan(i)
    gather(cuts - 1)
    for each in mix_copies:
        each.wait_recv()
    side.wait_recv()
    branch = alpha_mix * resid[...].astype(jnp.float32)
    for k in (p, partner):
        branch = branch + dot(token_rows[k], wb_all[k])
    for c in range(cuts):
        for j in steps:
            for o in range(n_x):
                onward(j, o, c).wait_recv()
    for j in steps:
        for k in (slot_of(j), partner + slot_of(j) - p):
            branch = branch + dot(token_rows[k], wb_all[k])
    blocks[z] = layer_norm(branch, ngain[...][None, :]).astype(jnp.bfloat16)
    for c in range(chunks):
        relay(z, c)

    dispatch(0)
    shared()
    for i in range(1, n_z):
        receive(i)
        dispatch(i)
    last = n_z - 1
    for i in range(last, 0, -1):
        experts(i)
    combine(last)
    pass_on(last)
    experts(0)
    for i in range(last - 1, 0, -1):
        combine(i)
        pass_on(i)
    combine(0)
    for c in range(chunks):
        take(0, z, c, z > 0)
        take(1, z, c, z + 1 < n_z)
    out_ref[...] = layer_norm(column[z], fgain[...][None, :]).astype(jnp.bfloat16)

    for zb in range(n_z):
        for c in range(chunks):
            src = blocks.at[zb, :, lane(c)]

            @pl.when(rises(zb))
            def _():
                up(src, zb, c).wait_send()

            @pl.when(sinks(zb))
            def _():
                down(src, zb, c).wait_send()

    for i in range(1, n_z):
        for c in range(chunks):
            link(0, near[i], c).wait_send()
    for i in range(n_z):
        for q in range(1, peers):
            go(i, q).wait_send()
            back(i, q).wait_send()
    halo_copy.wait_send()
    side.wait_send()
    for each in stat_copies + mix_copies:
        each.wait_send()
    for c in range(cuts):
        for j in steps:
            across(j, c).wait_send()
            onward(j, 0, c).wait_send()
            for o in range(1, n_x):
                along(j, o, c).wait_send()
                onward(j, o, c).wait_send()


def local(
    n_sp, n_tp,
    resid, pool_in, doc_ids, w_group, pool_scale, w_branch, norm_gain, route_ids, route_wts,
    w_exp_gate, w_exp_up, w_exp_down, w_sh_gate, w_sh_up, w_sh_down, final_gain,
):
    toks, width = pool_in.shape
    rows, model = resid.shape
    depth = w_branch.shape[0]
    top = route_ids.shape[1]
    cap = 2 * rows * top // (n_sp * n_tp)
    n_x = max(k for k in range(1, n_sp + 1) if n_sp % k == 0 and k * k <= n_sp)
    n_z = n_sp // n_x
    ff = w_sh_gate.shape[1]
    vmem, hbm = pl.BlockSpec(memory_space=pltpu.VMEM), pl.BlockSpec(memory_space=pl.ANY)
    dma = pltpu.SemaphoreType.DMA
    bf16, f32 = jnp.bfloat16, jnp.float32
    peers = n_x * n_tp
    seats = pltpu.VMEM((n_z, peers * cap, model), bf16)
    block = (rows, model)
    wide, tall = pltpu.VMEM((model, ff), bf16), pltpu.VMEM((ff, model), bf16)
    hops = n_tp // 2
    return pl.pallas_call(
        functools.partial(layer_kernel, n_sp, n_tp, n_x, cap, top),
        out_shape=jax.ShapeDtypeStruct(block, bf16),
        in_specs=[hbm] * 16,
        out_specs=vmem,
        scratch_shapes=[
            pltpu.VMEM((halo + toks, width), bf16),
            pltpu.VMEM(doc_ids.shape, jnp.int32),
            pltpu.VMEM(w_group.shape, bf16),
            pltpu.VMEM(pool_scale.shape, bf16),
            pltpu.VMEM((1, *pool_scale.shape), f32),
            pltpu.VMEM(block, bf16),
            pltpu.VMEM((model,), bf16),
            pltpu.VMEM((top, rows), jnp.int32),
            pltpu.VMEM((top, rows), f32),
            pltpu.VMEM((model,), bf16),
            pltpu.VMEM((n_sp, 8, width + 128 + rows), f32),
            pltpu.VMEM((toks, width), bf16),
            pltpu.VMEM((n_tp, rows, width), bf16),
            pltpu.VMEM((n_tp, depth, model), bf16),
            wide, wide, tall, wide, wide, tall,
            pltpu.VMEM((n_z, *block), bf16),
            seats, seats, seats,
            pltpu.VMEM((n_z, *block), f32),
            pltpu.VMEM((n_z, *block), bf16),
            pltpu.VMEM((2, n_z, *block), bf16),
            pltpu.VMEM(block, f32),
            pltpu.VMEM((n_z, peers * cap, rows), bf16), pltpu.VMEM((n_z, peers * cap, 2 * rows), bf16),
            dma((10,)), dma((n_sp,)), dma((n_sp,)), dma, dma, dma((n_tp,)), dma((n_tp,)),
            dma((hops, wb_cuts)), dma((hops, wb_cuts)),
            dma((hops, n_x, wb_cuts)), dma((hops, n_x, wb_cuts)), dma, dma,
            dma((hops, n_x, wb_cuts)), dma((hops, n_x, wb_cuts)),
            dma((6,)), dma((n_z, chunks)), dma((n_z, chunks)), dma((n_z, chunks)),
            dma((n_z, peers)), dma((n_z, peers)), dma((n_z, peers)), dma((n_z, peers)),
            dma((n_z, chunks)), dma((2, n_z, chunks)),
        ],
        compiler_params=pltpu.CompilerParams(
            collective_id=0, has_side_effects=True, vmem_limit_bytes=62 << 20
        ),
        name="pool_and_experts",
    )(
        pool_in, doc_ids, w_group, pool_scale, w_branch, resid, norm_gain, route_ids.T, route_wts.T,
        w_exp_gate, w_exp_up, w_exp_down, w_sh_gate, w_sh_up, w_sh_down, final_gain,
    )


def solution(mesh):
    both = P(("sp", "tp"), None)
    stack = P(("sp", "tp"), None, None)
    placed = (
        both, P("sp", "tp"), P("sp"), P(), P(), P("tp", None), P(), both, both,
        stack, stack, stack, P(), P(), P(), P(),
    )
    return jax.shard_map(
        functools.partial(local, mesh.shape["sp"], mesh.shape["tp"]),
        mesh=mesh, in_specs=placed, out_specs=both, check_vma=False,
    )
```

time: 156 us -> 133 us (0.85)
  Pallas kernels: 143 us -> 131 us
  local copies, waits for them, and re-layouts: 11.6 us -> 1.88 us
    pallas_call x2 -> x1, Pallas kernels: 143 us -> 131 us  [local(): pl.pallas_call(functools.partial(layer_kernel, n_sp, n_tp, n_x, cap, top)...]
    unnamed x15 -> x1, local copies, waits for them, and re-layouts: 8.11 us -> 1.88 us
    broadcast_in_dim x4 -> x0, local copies, waits for them, and re-layouts: 3.48 us -> none  [the longest x1 1.28 us: local(): final_gain[None, :]]
where the time goes in v2:
time: 133 us
  Pallas kernels  131 us (98%)
  local copies, waits for them, and re-layouts  1.88 us (1%)
    pallas_call x1, Pallas kernels, local(): pl.pallas_call(functools.partial(layer_kernel, n_sp, n_tp, n_x, cap, top)...  131 us

profile of v2, /device:TPU:0, one launch (start us, length us, event | category | flops | bytes accessed | tf_op | source)
XLA Modules:
  0.0 132.8 jit_solution(15656794506420951306)
XLA Ops:
  0.0 130.9 %pool_and_experts.1 = bf16[128,2048]{1,0:T(8,128)(2,1)} custom-call(bf16[512,256]{1,0:T(8,128)(2,1)} %pool_hbm.1, s32[512]{0:T(512)} %doc_hbm.1, bf16[8,128,128]{2,1,0:T(8,128)(2,1)} %wg_hbm.1, bf16[1024]{0:T(1024)(128)(2,1)} %scale_hbm.1, bf16[256,2048]{1,0:T(8,128)(2,1)} %wb_hbm.1, bf16[128,2048]{1,0:T(8,128)(2,1)} %resid_hbm.1, ...), custom_call_target="tpu_custom_call" | custom-call | tf_op jit(solution)/shard_map/pool_and_experts/pallas_call | solution.py:471
  130.9 1.9 %copy.18 = bf16[128,2048]{1,0:T(8,128)(2,1)} copy(bf16[128,2048]{1,0:T(8,128)(2,1)} %pool_and_experts.1) | data formatting | bytes 1048576

commit v3 on v2

--- a/solution.py
+++ b/solution.py
@@ -13,6 +13,7 @@
 halo = max(pool_windows)
 MESH = pl.DeviceIdType.MESH
 wb_cuts = 4
+sent_part = 4 / 8
 chunks = 4
 
 
@@ -35,11 +36,12 @@
     pool_hbm, doc_hbm, wg_hbm, scale_hbm, wb_hbm, resid_hbm, ngain_hbm, ids_hbm, wts_hbm,
     eg_hbm, eu_hbm, ed_hbm, sg_hbm, su_hbm, sd_hbm, fgain_hbm,
     out_ref,
-    ext, doc, wg, scales, flat, resid, ngain, ids, wts, fgain,
-    stats, mixed, token_rows, wb_all,
+    ext, doc, docx, wg, scales, flat, resid, ngain, ids, wts, fgain,
+    stats, mixed, token_rows, wb_all, lent, parts_out, parts_in,
     eg, eu, ed, sg, su, sd, blocks, outgoing, arrived, returned, column, partial, chain, acc, pick, share,
-    in_sem, stat_send, stat_recv, halo_send, halo_recv, mix_send, mix_recv,
+    in_sem, stat_send, stat_recv, halo_send, halo_recv, doc_send, doc_recv, mix_send, mix_recv,
     wby_send, wby_recv, wbx_send, wbx_recv, side_send, side_recv, fw_send, fw_recv,
+    lent_send, lent_recv, part_send, part_recv,
     load_sem, up_send, down_send, block_recv, go_send, go_recv, back_send, back_recv,
     chain_send, chain_recv,
 ):
@@ -56,6 +58,7 @@
     piece = depth // n_x
     cuts = max(1, min(wb_cuts, piece // 32))
     cut = piece // cuts
+    kept = model - parts_in.shape[2]
 
     def mate(q):
         return z * n_x + lax.rem(x + q // n_tp, n_x), lax.rem(p + q % n_tp, n_tp)
@@ -215,7 +218,7 @@
         return pl.ds(pl.multiple_of(at * piece + c * cut, cut), cut)
 
     def wb_copy(slot, at, c, send, recv, where):
-        src = wb_all.at[slot, wb_rows(at, c)]
+        src = wb_all.at[slot, wb_rows(at, c), pl.ds(0, kept)]
         return copy(src, src, send, recv, where)
 
     def across(j, c):
@@ -235,6 +238,8 @@
     steps = range(1, n_tp // 2)
 
     def spread(c):
+        if c >= cuts:
+            return
         for j in steps:
             across(j, c).wait_recv()
             for o in range(1, n_x):
@@ -242,10 +247,24 @@
             onward(j, 0, c).start()
 
     def gather(c):
+        if not 0 <= c < cuts:
+            return
         for j in steps:
             for o in range(1, n_x):
                 along(j, o, c).wait_recv()
                 onward(j, o, c).start()
+
+    def block_rows(q):
+        return pl.ds(pl.multiple_of(q * rows, rows), rows)
+
+    def lend(j):
+        q = lax.rem(partner + 2 * j, n_tp)
+        return copy(mixed.at[block_rows(q)], lent.at[j], lent_send.at[j], lent_recv.at[j], (s, partner))
+
+    def part(j):
+        return copy(
+            parts_out.at[j], parts_in.at[j], part_send.at[j], part_recv.at[j], (s, lax.rem(p + 2 * j, n_tp))
+        )
 
     side = copy(wb_all.at[p], wb_all.at[p], side_send, side_recv, (s, partner))
     halo_copy = copy(
@@ -255,20 +274,15 @@
         copy(stats.at[s], stats.at[s], stat_send.at[k], stat_recv.at[k], (lax.rem(s + k, n_sp), p))
         for k in range(1, n_sp)
     ]
-    inputs[0].wait()
-    pl.semaphore_wait(barrier, n_sp - 1 + n_x * (n_tp - 1))
-    for c in range(cuts):
-        for j in steps:
-            across(j, c).start()
-    side.start()
+    doc_copy = copy(
+        docx.at[:, pl.ds(toks, halo)], docx.at[:, pl.ds(0, halo)], doc_send, doc_recv, (lax.rem(s + 1, n_sp), p)
+    )
     for load in inputs[1:5]:
         load.wait()
-    halo_copy.start()
-
     values = ext[halo:, :]
-    docr = doc[...][None, :]
-    docc = jnp.transpose(jnp.broadcast_to(docr.astype(jnp.float32), (128, toks)))[:, 0:1]
-    docr = docr.astype(jnp.float32)
+    docr = doc[...][None, :].astype(jnp.float32)
+    docx[0:1, halo:] = docr
+    docc = jnp.transpose(jnp.broadcast_to(docr, (128, toks)))[:, 0:1]
     last = jnp.max(docr, axis=1, keepdims=True)
     first = jnp.min(docr, axis=1, keepdims=True)
     tail = (docr == last).astype(jnp.float32)
@@ -279,20 +293,45 @@
     stats[s, 0:top, width + 128 :] = ids[...].astype(jnp.float32)
     stats[s, top : 2 * top, width + 128 :] = wts[...]
     stats[s, :, width : width + 128] = jnp.where(lane_at == 0, last, tail_count)
+    inputs[0].wait()
+    pl.semaphore_wait(barrier, n_sp - 1 + n_x * (n_tp - 1))
+    for c in range(cuts):
+        for j in steps:
+            across(j, c).start()
     for each in stat_copies:
         each.start()
-    for load in loads:
-        load.start()
+    doc_copy.start()
+    halo_copy.start()
+    side.start()
 
     tpos = lax.broadcasted_iota(jnp.int32, (toks, toks), 0)
     spos = lax.broadcasted_iota(jnp.int32, (toks, toks), 1)
     same = ((docc == docr) & (spos <= tpos)).astype(jnp.float32)
     here = jnp.sum(same, axis=1, keepdims=True)
     running = dot(same.astype(jnp.bfloat16), values)
+    groups = width // group_width
+    for load in inputs[5:]:
+        load.wait()
+    flat[...] = scales[...].astype(jnp.float32)[None, :]
+    tpos = lax.broadcasted_iota(jnp.int32, (toks, toks + halo), 0) + halo
+    spos = lax.broadcasted_iota(jnp.int32, (toks, toks + halo), 1)
+    away = tpos - spos
+    doc_copy.wait_recv()
+    halo_copy.wait_recv()
+    held = (docc == docx[...]) & (away >= 0) & (spos >= jnp.where(s == 0, halo, 0))
+    windows, recents = [], []
+    for i in range(groups):
+        window = jnp.int32(0)
+        for at, size in enumerate(pool_windows):
+            window = jnp.where(p * groups + i == at, size, window)
+        band = (held & (away < window)).astype(jnp.float32).astype(jnp.bfloat16)
+        windows.append(window.astype(jnp.float32))
+        recents.append(dot(band, ext[:, i * group_width : (i + 1) * group_width]))
     spread(0)
 
     for each in stat_copies:
         each.wait_recv()
+    spread(1)
     prev_count = jnp.zeros((1, 1), jnp.float32)
     prev_sums = jnp.zeros((1, width), jnp.float32)
     for k in range(n_sp):
@@ -304,30 +343,17 @@
     length = here + jnp.where(carried, prev_count, 0.0)
     running = running + jnp.where(carried, prev_sums, 0.0)
     doc_mean = running / length
-
-    halo_copy.wait_recv()
-    for load in inputs[5:]:
-        load.wait()
-    if cuts > 1:
-        spread(1)
-    tpos = lax.broadcasted_iota(jnp.int32, (toks, toks + halo), 0) + halo
-    spos = lax.broadcasted_iota(jnp.int32, (toks, toks + halo), 1)
-    away = tpos - spos
-    groups = width // group_width
-    flat[...] = scales[...].astype(jnp.float32)[None, :]
     for i in range(groups):
         g = p * groups + i
-        window = jnp.int32(0)
-        for at, size in enumerate(pool_windows):
-            window = jnp.where(g == at, size, window)
-        span = jnp.minimum(length, window.astype(jnp.float32))
-        band = ((away >= 0) & (away < span.astype(jnp.int32))).astype(jnp.float32).astype(jnp.bfloat16)
         cols = slice(i * group_width, (i + 1) * group_width)
-        recent = dot(band, ext[:, cols])
-        offset = 0.5 * (recent / span + doc_mean[:, cols]) - values[:, cols].astype(jnp.float32)
+        recent = recents[i] / jnp.minimum(length, windows[i])
+        offset = 0.5 * (recent + doc_mean[:, cols]) - values[:, cols].astype(jnp.float32)
         turned = dot(offset.astype(jnp.bfloat16), wg[g])
         scale = flat[0:1, pl.ds(pl.multiple_of(g * group_width, group_width), group_width)]
         mixed[:, cols] = (turned * scale).astype(jnp.bfloat16)
+    spread(2)
+    for j in steps:
+        lend(j).start()
 
     mix_copies = []
     for k in range(1, n_tp):
@@ -340,9 +366,20 @@
         )
         mix_copies[-1].start()
     token_rows[p] = mixed[pl.ds(pl.multiple_of(p * rows, rows), rows), :]
-    for c in range(2, cuts):
+
+    for c in range(3, cuts):
         spread(c)
-        gather(c - 2)
+    side.wait_recv()
+    for load in loads:
+        load.start()
+    for j in steps:
+        lend(j).wait_recv()
+        mine = mixed[block_rows(lax.rem(p + 2 * j, n_tp)), :]
+        total = dot(mine, wb_all[p, :, kept:]) + dot(lent[j], wb_all[partner, :, kept:])
+        parts_out[j] = total.astype(jnp.bfloat16)
+        part(j).start()
+    gather(0)
+    gather(1)
 
     expert_at = [z * n_x * n_tp + lax.rem(x + q // n_tp, n_x) * n_tp + lax.rem(p + q % n_tp, n_tp) for q in range(peers)]
     earlier = lax.broadcasted_iota(jnp.int32, (rows, rows), 0) < lax.broadcasted_iota(jnp.int32, (rows, rows), 1)
@@ -373,14 +410,11 @@
             share[zb, seat(q), rows:] = (full - high.astype(jnp.float32)).astype(jnp.bfloat16)
 
     plan(0)
-    if cuts > 1:
-        gather(cuts - 2)
-    for i in range(1, n_z):
-        plan(i)
-    gather(cuts - 1)
+    gather(2)
+    for c in range(3, cuts):
+        gather(c)
     for each in mix_copies:
         each.wait_recv()
-    side.wait_recv()
     branch = alpha_mix * resid[...].astype(jnp.float32)
     for k in (p, partner):
         branch = branch + dot(token_rows[k], wb_all[k])
@@ -388,14 +422,21 @@
         for j in steps:
             for o in range(n_x):
                 onward(j, o, c).wait_recv()
+    left, right = branch[:, :kept], branch[:, kept:]
     for j in steps:
         for k in (slot_of(j), partner + slot_of(j) - p):
-            branch = branch + dot(token_rows[k], wb_all[k])
+            left = left + dot(token_rows[k], wb_all[k, :, :kept])
+    for j in steps:
+        part(j).wait_recv()
+        right = right + parts_in[j].astype(jnp.float32)
+    branch = jnp.concatenate([left, right], axis=1)
     blocks[z] = layer_norm(branch, ngain[...][None, :]).astype(jnp.bfloat16)
     for c in range(chunks):
         relay(z, c)
 
     dispatch(0)
+    for i in range(1, n_z):
+        plan(i)
     shared()
     for i in range(1, n_z):
         receive(i)
@@ -435,6 +476,10 @@
             go(i, q).wait_send()
             back(i, q).wait_send()
     halo_copy.wait_send()
+    doc_copy.wait_send()
+    for j in steps:
+        lend(j).wait_send()
+        part(j).wait_send()
     side.wait_send()
     for each in stat_copies + mix_copies:
         each.wait_send()
@@ -468,6 +513,7 @@
     block = (rows, model)
     wide, tall = pltpu.VMEM((model, ff), bf16), pltpu.VMEM((ff, model), bf16)
     hops = n_tp // 2
+    summed = model - int(model * sent_part) // 128 * 128
     return pl.pallas_call(
         functools.partial(layer_kernel, n_sp, n_tp, n_x, cap, top),
         out_shape=jax.ShapeDtypeStruct(block, bf16),
@@ -476,6 +522,7 @@
         scratch_shapes=[
             pltpu.VMEM((halo + toks, width), bf16),
             pltpu.VMEM(doc_ids.shape, jnp.int32),
+            pltpu.VMEM((1, halo + toks), f32),
             pltpu.VMEM(w_group.shape, bf16),
             pltpu.VMEM(pool_scale.shape, bf16),
             pltpu.VMEM((1, *pool_scale.shape), f32),
@@ -488,6 +535,8 @@
             pltpu.VMEM((toks, width), bf16),
             pltpu.VMEM((n_tp, rows, width), bf16),
             pltpu.VMEM((n_tp, depth, model), bf16),
+            pltpu.VMEM((hops, rows, width), bf16),
+            pltpu.VMEM((hops, rows, summed), bf16), pltpu.VMEM((hops, rows, summed), bf16),
             wide, wide, tall, wide, wide, tall,
             pltpu.VMEM((n_z, *block), bf16),
             seats, seats, seats,
@@ -496,10 +545,11 @@
             pltpu.VMEM((2, n_z, *block), bf16),
             pltpu.VMEM(block, f32),
             pltpu.VMEM((n_z, peers * cap, rows), bf16), pltpu.VMEM((n_z, peers * cap, 2 * rows), bf16),
-            dma((10,)), dma((n_sp,)), dma((n_sp,)), dma, dma, dma((n_tp,)), dma((n_tp,)),
+            dma((10,)), dma((n_sp,)), dma((n_sp,)), dma, dma, dma, dma, dma((n_tp,)), dma((n_tp,)),
             dma((hops, wb_cuts)), dma((hops, wb_cuts)),
             dma((hops, n_x, wb_cuts)), dma((hops, n_x, wb_cuts)), dma, dma,
             dma((hops, n_x, wb_cuts)), dma((hops, n_x, wb_cuts)),
+            dma((hops,)), dma((hops,)), dma((hops,)), dma((hops,)),
             dma((6,)), dma((n_z, chunks)), dma((n_z, chunks)), dma((n_z, chunks)),
             dma((n_z, peers)), dma((n_z, peers)), dma((n_z, peers)), dma((n_z, peers)),
             dma((n_z, chunks)), dma((2, n_z, chunks)),

time: 133 us -> 129 us (0.970); the launches traced: 133 us -> 127 us
  Pallas kernels: 131 us -> 125 us
    pallas_call x1, Pallas kernels: 131 us -> 125 us  [local(): pl.pallas_call(functools.partial(layer_kernel, n_sp, n_tp, n_x, cap, top)...]
where the time goes in v3:
time: 129 us; the launch traced here: 127 us
  Pallas kernels  125 us (97%)
  local copies, waits for them, and re-layouts  1.88 us (1%)
    pallas_call x1, Pallas kernels, local(): pl.pallas_call(functools.partial(layer_kernel, n_sp, n_tp, n_x, cap, top)...  125 us

profile of v3, /device:TPU:0, one launch (start us, length us, event | category | flops | bytes accessed | tf_op | source)
XLA Modules:
  0.0 127.3 jit_solution(1535214582410494812)
XLA Ops:
  0.0 125.4 %pool_and_experts.1 = bf16[128,2048]{1,0:T(8,128)(2,1)} custom-call(bf16[512,256]{1,0:T(8,128)(2,1)} %pool_hbm.1, s32[512]{0:T(512)} %doc_hbm.1, bf16[8,128,128]{2,1,0:T(8,128)(2,1)} %wg_hbm.1, bf16[1024]{0:T(1024)(128)(2,1)} %scale_hbm.1, bf16[256,2048]{1,0:T(8,128)(2,1)} %wb_hbm.1, bf16[128,2048]{1,0:T(8,128)(2,1)} %resid_hbm.1, ...), custom_call_target="tpu_custom_call" | custom-call | tf_op jit(solution)/shard_map/pool_and_experts/pallas_call | solution.py:517
  125.4 1.9 %copy.18 = bf16[128,2048]{1,0:T(8,128)(2,1)} copy(bf16[128,2048]{1,0:T(8,128)(2,1)} %pool_and_experts.1) | data formatting | bytes 1048576
